TPU v7x, 32 devices: a whole 2x2x4 slice. The times are simulated.
32 devices in a mesh: sp: 4 (over z), tp: 8 (over y, x, core).
Axes of the slice: x: 2, y: 2, z: 4, core: 2. Of those that a mesh axis runs over, the one named last changes fastest.
Arguments:
- latent: bfloat16 [2048, 4096], P(('sp', 'tp')), may hold values from -6 to 6
- context: bfloat16 [512, 4096], P('sp'), may hold values from -6 to 6
- condition: float32 [4096], P('sp'), may hold values from -6 to 6
- context_cond: float32 [4096], P('sp'), may hold values from -6 to 6
- mod_weight: bfloat16 [4096, 12288], P('sp', 'tp'), may hold values from -0.09375 to 0.09375
- norm_gain: float32 [4096], replicated, may hold values from 0.1 to 1.9
- query_weight: bfloat16 [4096, 4096], P(None, 'tp'), may hold values from -0.09375 to 0.09375
- key_weight: bfloat16 [4096, 2048], P(None, 'tp'), may hold values from -0.09375 to 0.09375
- value_weight: bfloat16 [4096, 2048], P(None, 'tp'), may hold values from -0.09375 to 0.09375
- out_weight: bfloat16 [4096, 4096], P(None, 'tp'), may hold values from -0.375 to 0.375
- query_gain: float32 [64], replicated, may hold values from 1.2 to 6
- key_gain: float32 [64], replicated, may hold values from 1.2 to 6
- context_lift: float32 [64], P('tp'), may hold values from 0.5 to 2
Outputs:
- updated: bfloat16 [2048, 4096], P(('sp', 'tp'))
All inputs are finite; a program needn't handle non-finite values.
Results may differ from a plain program's by a relative error of at most 0.0085.
The roundings to bfloat16 on the way count: a program that leaves them out, or rounds other values in their place, can miss the bound.
Values may be sent and summed in bfloat16 or wider, within the bound.
A program may use at most 64 MiB of HBM per device.

v0:
```python
import jax
import jax.numpy as jnp
from jax import lax
from jax.sharding import PartitionSpec as P

GRID_W = 64
EPS = 1e-06


def modulate(row_block, gain_vec, mod_row, model_width):
    row_values = row_block.astype(jnp.float32)
    normal = row_values * lax.rsqrt(jnp.mean(row_values * row_values, axis=-1, keepdims=True) + EPS)
    shift_part = mod_row[:model_width]
    scale_part = mod_row[model_width : 2 * model_width]
    return (normal * gain_vec * (1.0 + scale_part) + shift_part).astype(jnp.bfloat16)


def head_norm(values, gain_vec):
    return values * lax.rsqrt(jnp.mean(values * values, axis=-1, keepdims=True) + EPS) * gain_vec


def rope_tables(positions, head_size):
    freq_count = head_size // 4
    inverse = 10000.0 ** (-jnp.arange(freq_count, dtype=jnp.float32) / freq_count)
    grid_row = (positions // GRID_W).astype(jnp.float32)
    grid_col = (positions % GRID_W).astype(jnp.float32)
    angles = jnp.concatenate([grid_row[:, None] * inverse, grid_col[:, None] * inverse], axis=-1)
    return (jnp.cos(angles), jnp.sin(angles))


def rotate(values, cos_table, sin_table):
    paired = values.reshape(values.shape[:-1] + (values.shape[-1] // 2, 2))
    even_part = paired[..., 0]
    odd_part = paired[..., 1]
    cos_wide = cos_table[:, None, :]
    sin_wide = sin_table[:, None, :]
    turned = jnp.stack(
        [even_part * cos_wide - odd_part * sin_wide, even_part * sin_wide + odd_part * cos_wide],
        axis=-1,
    )
    return turned.reshape(values.shape)


def local(
    latent,
    context,
    condition,
    context_cond,
    mod_weight,
    norm_gain,
    query_weight,
    key_weight,
    value_weight,
    out_weight,
    query_gain,
    key_gain,
    context_lift,
):
    model_width = latent.shape[1]
    head_size = query_gain.shape[0]
    query_count = query_weight.shape[1] // head_size
    kv_count = key_weight.shape[1] // head_size
    group_size = query_count // kv_count
    score_scale = head_size ** (-0.5)
    cond_pair = jax.nn.silu(jnp.stack([condition, context_cond])).astype(jnp.bfloat16)
    partial_mod = jnp.dot(cond_pair, mod_weight, preferred_element_type=jnp.float32)
    summed_mod = lax.psum(partial_mod, "sp")
    modulation = lax.all_gather(summed_mod, "tp", axis=1, tiled=True)
    normed = modulate(latent, norm_gain, modulation[0], model_width)
    block_first = lax.axis_index("sp") * (latent.shape[0] * lax.axis_size("tp"))
    gathered = lax.all_gather(normed, "tp", axis=0, tiled=True)
    row_count = gathered.shape[0]
    query_raw = jnp.dot(gathered, query_weight, preferred_element_type=jnp.float32)
    key_raw = jnp.dot(gathered, key_weight, preferred_element_type=jnp.float32)
    value_raw = jnp.dot(gathered, value_weight, preferred_element_type=jnp.float32)
    positions = block_first + jnp.arange(row_count, dtype=jnp.int32)
    cos_table, sin_table = rope_tables(positions, head_size)
    query_rot = rotate(
        head_norm(query_raw.reshape(row_count, query_count, head_size), query_gain),
        cos_table,
        sin_table,
    )
    key_rot = rotate(
        head_norm(key_raw.reshape(row_count, kv_count, head_size), key_gain), cos_table, sin_table
    )
    joined = jnp.concatenate(
        [
            query_rot.reshape(row_count, -1).astype(jnp.bfloat16),
            key_rot.reshape(row_count, -1).astype(jnp.bfloat16),
            value_raw.astype(jnp.bfloat16),
        ],
        axis=1,
    )
    query_cols = query_count * head_size
    kv_cols = kv_count * head_size
    queries = joined[:, :query_cols]
    keys_here = joined[:, query_cols : query_cols + kv_cols]
    values_here = joined[:, query_cols + kv_cols :]
    normed_ctx = modulate(context, norm_gain, modulation[1], model_width)
    key_raw = jnp.dot(normed_ctx, key_weight, preferred_element_type=jnp.float32)
    ctx_key = head_norm(key_raw.reshape(context.shape[0], kv_count, head_size), key_gain)
    ctx_value = jnp.dot(normed_ctx, value_weight, preferred_element_type=jnp.float32)
    own_keys = ctx_key.reshape(context.shape[0], -1).astype(jnp.bfloat16)
    own_values = ctx_value.astype(jnp.bfloat16)
    ctx_keys, ctx_values = (
        lax.all_gather(own_keys, "sp", axis=0, tiled=True),
        lax.all_gather(own_values, "sp", axis=0, tiled=True),
    )
    query_rows = queries.shape[0]
    grouped = queries.reshape(query_rows, kv_count, group_size, head_size)
    lift_rows = context_lift.reshape(kv_count, group_size)
    zero_lift = jnp.zeros_like(lift_rows)

    def absorb(carry_state, key_block, value_block, offset):
        running_max, denom, numer = carry_state
        key_heads = key_block.reshape(-1, kv_count, head_size)
        value_heads = value_block.reshape(-1, kv_count, head_size)
        scores = jnp.einsum(
            "qhgd,khd->hgqk", grouped, key_heads, preferred_element_type=jnp.float32
        )
        scores = scores * score_scale + offset[:, :, None, None]
        new_max = jnp.maximum(running_max, jnp.max(scores, axis=-1))
        expo = jnp.exp(scores - new_max[..., None])
        rescale = jnp.exp(running_max - new_max)
        denom = denom * rescale + jnp.sum(expo, axis=-1)
        numer = numer * rescale[..., None] + jnp.einsum(
            "hgqk,khd->hgqd",
            expo.astype(jnp.bfloat16),
            value_heads,
            preferred_element_type=jnp.float32,
        )
        return (new_max, denom, numer)

    def sweep(carry_state, key_rows, value_rows, offset):
        row_count = key_rows.shape[0]
        block_size = 512
        if block_size == row_count:
            return absorb(carry_state, key_rows, value_rows, offset)
        key_blocks = key_rows.reshape(row_count // block_size, block_size, -1)
        value_blocks = value_rows.reshape(row_count // block_size, block_size, -1)

        def absorb_block(state_now, key_value):
            return (absorb(state_now, key_value[0], key_value[1], offset), None)

        final_state, unused = lax.scan(absorb_block, carry_state, (key_blocks, value_blocks))
        return final_state

    initial = (
        jnp.full((kv_count, group_size, query_rows), -jnp.inf, jnp.float32),
        jnp.zeros((kv_count, group_size, query_rows), jnp.float32),
        jnp.zeros((kv_count, group_size, query_rows, head_size), jnp.float32),
    )
    after_context = sweep(initial, ctx_keys, ctx_values, lift_rows)
    gathered = (
        lax.all_gather(keys_here, "sp", axis=0, tiled=True),
        lax.all_gather(values_here, "sp", axis=0, tiled=True),
    )
    running_max, denom, numer = sweep(after_context, gathered[0], gathered[1], zero_lift)
    attended = (numer / denom[..., None]).astype(jnp.bfloat16)
    attended = attended.transpose(2, 0, 1, 3).reshape(query_rows, query_cols)
    mixed_cols = jnp.dot(
        lax.all_gather(attended, "tp", axis=1, tiled=True),
        out_weight,
        preferred_element_type=jnp.float32,
    )
    mixed_rows = lax.all_to_all(
        mixed_cols.astype(jnp.bfloat16), "tp", split_axis=0, concat_axis=1, tiled=True
    )
    gate_lat = modulation[0, 2 * model_width :]
    return (latent.astype(jnp.float32) + gate_lat * mixed_rows.astype(jnp.float32)).astype(
        jnp.bfloat16
    )


def solution(mesh):
    return jax.shard_map(
        local,
        mesh=mesh,
        in_specs=(
            P(("sp", "tp"), None),
            P("sp", None),
            P("sp"),
            P("sp"),
            P("sp", "tp"),
            P(),
            P(None, "tp"),
            P(None, "tp"),
            P(None, "tp"),
            P(None, "tp"),
            P(),
            P(),
            P("tp"),
        ),
        out_specs=P(("sp", "tp"), None),
        check_vma=False,
    )
```

profile of v0, /device:TPU:0, one launch (start us, length us, event | category | flops | bytes accessed | tf_op | source)
XLA Modules:
  0.0 258.7 jit_solution(14006119027118180818)
XLA Ops:
  6.6 1.4 fusion.24
  8.6 1.2 fusion.36
  9.8 20.4 %psum.7 = f32[2,1536]{1,0:T(2,128)S(1)} all-reduce(f32[2,1536]{1,0:T(2,128)S(1)} %fusion.36), channel_id=1, replica_groups=mesh['sp'=4,'tp'=8] {'sp'}, use_global_device_ids=true, to_apply=%region_0.1 | all-reduce | flops 3072 | bytes 24576 | tf_op jit(solution)/shard_map/psum | solution.py:67
  30.3 9.2 %all_gather.21 = f32[2,12288]{1,0:T(2,128)S(1)} all-gather(f32[2,1536]{1,0:T(2,128)S(1)} %psum.7), channel_id=1, replica_groups=mesh['sp'=4,'tp'=8] {'tp'}, dimensions={1}, use_global_device_ids=true | all-gather | bytes 110592 | tf_op jit(solution)/shard_map/all_gather | solution.py:68
  40.2 2.1 fusion.28
  44.0 1.5 fusion.16
  45.5 2.7 %convolution_convert_fusion.2 = bf16[128,256]{1,0:T(8,128)(2,1)S(1)} fusion(bf16[4096,256]{1,0:T(8,128)(2,1)} %param.23, bf16[128,4096]{1,0:T(8,128)(2,1)} %param.16, f32[4096]{0:T(1024)S(1)} %bitcast.146, f32[4096]{0:T(1024)S(1)} %bitcast.148, f32[4096]{0:T(1024)S(1)} %copy-done.7, f32[128]{0:T(128)S(1)} %add_rsqrt_fusion.4), kind=kOutput, calls=%fused_computation.34 | convolution fusion | flops 271613952 | bytes 3260928 | tf_op jit(solution)/shard_map/dot_general | solution.py:102
  48.2 14.4 %all_gather.24 = bf16[512,256]{1,0:T(8,128)(2,1)S(1)} all-gather(bf16[128,256]{1,0:T(8,128)(2,1)S(1)} %convolution_convert_fusion.2), channel_id=1, replica_groups=mesh['sp'=4,'tp'=8] {'sp'}, dimensions={0}, use_global_device_ids=true | all-gather | bytes 327680 | tf_op jit(solution)/shard_map/all_gather | solution.py:107
  62.6 0.8 copy.34
  63.4 2.5 fusion.49
  66.3 14.6 %all_gather.22 = bf16[512,256]{1,0:T(8,128)(2,1)} all-gather(bf16[128,256]{1,0:T(8,128)(2,1)S(1)} %multiply_convert_fusion), channel_id=1, replica_groups=mesh['sp'=4,'tp'=8] {'sp'}, dimensions={0}, use_global_device_ids=true | all-gather | bytes 327680 | tf_op jit(solution)/shard_map/all_gather | solution.py:106
  80.9 1.1 copy.33
  82.3 5.0 %bitcast_reduce_fusion.3 = (f32[512,4]{0,1:T(4,128)S(1)}, f32[512,256]{0,1:T(8,128)}) fusion(bf16[512,4096]{1,0:T(8,128)(2,1)} %all-gather.5.cloned.1.call-done, bf16[4096,256]{1,0:T(8,128)(2,1)} %param.22), kind=kOutput, calls=%fused_computation.46 | convolution fusion | flops 1074001920 | bytes 6823936 | tf_op jit(solution)/shard_map/dot_general | solution.py:74
  87.3 2.2 reshape.207
  89.5 1.3 multiply_multiply_fusion.1
  91.5 1.3 pad_maximum_fusion.1
  92.7 1.8 convert_element_type.83
  94.7 7.4 %bitcast_reduce_fusion.2 = (f32[512,8]{0,1:T(8,128)}, f32[512,512]{0,1:T(8,128)}) fusion(bf16[512,4096]{1,0:T(8,128)(2,1)} %all-gather.5.cloned.1.call-done, bf16[4096,512]{1,0:T(8,128)(2,1)} %param.21), kind=kOutput, calls=%fused_computation.41 | convolution fusion | flops 2148003840 | bytes 9453568 | tf_op jit(solution)/shard_map/dot_general | solution.py:73
  102.2 2.8 %reshape.205 = f32[512,8,32,2]{0,3,2,1:T(2,128)} reshape(f32[512,512]{0,1:T(8,128)} %get-tuple-element.104) | data formatting | bytes 2097152 | tf_op jit(solution)/shard_map/reshape | solution.py:79
  105.0 0.7 add_rsqrt_fusion
  105.7 1.7 multiply_multiply_fusion
  107.5 1.4 subtract_convert_fusion
  108.8 2.0 pad_maximum_fusion
  110.8 2.1 convert_element_type.80
  112.9 4.8 %convolution_convert_fusion.1 = bf16[512,256]{1,0:T(8,128)(2,1)} fusion(bf16[512,4096]{1,0:T(8,128)(2,1)} %all-gather.5.cloned.1.call-done, bf16[4096,256]{1,0:T(8,128)(2,1)} %param.23), kind=kOutput, calls=%fused_computation.33 | convolution fusion | flops 1073872896 | bytes 6553600 | tf_op jit(solution)/shard_map/dot_general | solution.py:75
  118.0 2.5 bitcast_reduce_fusion.1
  120.6 1.7 fusion.13
  122.4 2.9 %fusion.21 = f32[4,2,512,64]{2,3,1,0:T(8,128)} fusion(bf16[512,4,64,1]{0,2,3,1:T(8,128)(2,1)S(1)} %bitcast.142, f32[4,512,512,2]{2,1,3,0:T(8,128)S(1)} %get-tuple-element.106, f32[4,2,512]{2,1,0:T(2,128)S(1)} %get-tuple-element.171, f32[4,2]{1,0:T(4,128)S(1)} %add.177, f32[4,2,512]{2,1,0:T(2,128)S(1)} %get-tuple-element.97), kind=kOutput, calls=%fused_computation.31 | convolution fusion | flops 277086208 | bytes 9732128 | tf_op jit(solution)/shard_map/hgqk,khd->hgqd/dot_general | solution.py:126
  125.2 2.3 copy.36
  127.5 21.5 %all-gather.9.cloned.1.call-done = bf16[2048,256]{1,0:T(8,128)(2,1)} async-done(((bf16[512,256]{1,0:T(8,128)(2,1)}), bf16[2048,256]{1,0:T(8,128)(2,1)}) %all-gather.9.cloned.1.call-update) | async-done | bytes 1048592 | tf_op jit(solution)/shard_map/all_gather | solution.py:156
  149.0 45.5 %while.14 = (s32[]{:T(128)}, f32[4,2,512]{2,1,0:T(2,128)S(1)}, f32[4,2,512]{2,1,0:T(2,128)S(1)}, f32[4,2,512,64]{2,3,1,0:T(8,128)}, bf16[4,512,256]{2,1,0:T(8,12...) while((s32[]{:T(128)}, f32[4,2,512]{2,1,0:T(2,128)S(1)}, ...), condition=%wide.region_11.12_spmd, body=%wide.region_8.11_spmd.sunk | while | flops 554180608 | bytes 40108212 | solution.py:145
  149.0 1.8 constant_dynamic-slice_fusion.3
  150.9 1.1 copy.51
  152.0 1.8 copy.52
  153.8 2.4 bitcast_reduce_fusion.6
  156.2 1.4 fusion.77
  157.6 1.8 fusion.78
  159.4 1.0 copy-done.2
  160.4 1.8 constant_dynamic-slice_fusion.3
  162.2 1.1 copy.51
  163.3 1.8 copy.52
  165.1 2.3 bitcast_reduce_fusion.6
  167.5 1.4 fusion.77
  169.0 1.8 fusion.78
  170.8 1.0 copy-done.2
  171.8 1.8 constant_dynamic-slice_fusion.3
  173.6 1.1 copy.51
  174.7 1.8 copy.52
  176.5 2.3 bitcast_reduce_fusion.6
  178.9 1.4 fusion.77
  180.3 1.8 fusion.78
  182.2 1.0 copy-done.2
  183.1 1.8 constant_dynamic-slice_fusion.3
  185.0 1.1 copy.51
  186.1 1.8 copy.52
  187.9 2.3 bitcast_reduce_fusion.6
  190.3 1.4 fusion.77
  191.7 1.8 fusion.78
  193.5 1.0 copy-done.2
  194.5 2.1 divide_convert_fusion
  196.7 36.1 %all-gather.11.cloned.1.call-done = bf16[512,4096]{0,1:T(8,128)(2,1)} async-done(((bf16[512,512]{0,1:T(8,128)(2,1)}), bf16[512,4096]{0,1:T(8,128)(2,1)}) %all-gather.11.cloned.1.call-update) | async-done | bytes 4194320 | tf_op jit(solution)/shard_map/all_gather | solution.py:162
  232.8 5.8 %convolution_convert_fusion = bf16[512,512]{1,0:T(8,128)(2,1)S(1)} fusion(bf16[512,4096]{0,1:T(8,128)(2,1)} %all-gather.11.cloned.1.call-done, bf16[4096,512]{1,0:T(8,128)(2,1)} %param.24), kind=kOutput, calls=%fused_computation.32 | convolution fusion | flops 2147745792 | bytes 8912896 | tf_op jit(solution)/shard_map/dot_general | solution.py:161
  238.6 12.4 %all_to_all.13 = bf16[8,64,512]{2,1,0:T(8,128)(2,1)S(1)} all-to-all(bf16[8,64,512]{2,1,0:T(8,128)(2,1)S(1)} %bitcast.140), channel_id=1, replica_groups=mesh['sp'=4,'tp'=8] {'tp'}, dimensions={0} | all-to-all | bytes 1048576 | tf_op jit(solution)/shard_map/all_to_all | solution.py:166
  251.2 0.9 fusion.29
  (85 shorter events, 5.2 us)
Async XLA Ops:
  6.5 2.1 copy-start
  6.5 39.0 %copy-start.7 = (f32[4096]{0:T(1024)S(1)}, f32[4096]{0:T(1024)}, u32[]{:S(2)}) copy-start(f32[4096]{0:T(1024)} %param.20) | copy-start | bytes 49156
  6.5 35.8 %copy-start.11 = (f32[8]{0:T(128)S(1)}, f32[8]{0:T(128)}, u32[]{:S(2)}) copy-start(f32[8]{0:T(128)} %param.27) | copy-start | bytes 100
  6.5 35.9 %copy-start.10 = (f32[64]{0:T(128)S(1)}, f32[64]{0:T(128)}, u32[]{:S(2)}) copy-start(f32[64]{0:T(128)} %param.26) | copy-start | bytes 772
  6.5 36.7 %copy-start.12 = (f32[64]{0:T(128)S(1)}, f32[64]{0:T(128)}, u32[]{:S(2)}) copy-start(f32[64]{0:T(128)} %param.25) | copy-start | bytes 772
  6.5 75.8 %all-gather.5.cloned.1.call-start = ((), (), s32[]{:S(2)}) async-start(), calls=%async_computation.1 | async-start | bytes 4718592 | tf_op jit(solution)/shard_map/all_gather | solution.py:71
  40.2 22.4 %copy-start.8 = (f32[1,4096]{1,0:T(1,128)}, f32[1,4096]{1,0:T(1,128)S(1)}, u32[]{:S(2)}) copy-start(f32[1,4096]{1,0:T(1,128)S(1)} %get-tuple-element.93) | copy-start | bytes 49156
  40.2 22.4 %copy-start.9 = (f32[1,4096]{1,0:T(1,128)}, f32[1,4096]{1,0:T(1,128)S(1)}, u32[]{:S(2)}) copy-start(f32[1,4096]{1,0:T(1,128)S(1)} %get-tuple-element.94) | copy-start | bytes 49156
  42.3 82.9 %all-gather.7.cloned.1.call-start = ((), (), s32[]{:S(2)}) async-start(), calls=%async_computation.2 | async-start | bytes 1310720 | tf_op jit(solution)/shard_map/all_gather | solution.py:155
  94.5 54.5 %all-gather.9.cloned.1.call-start = ((), (), s32[]{:S(2)}) async-start(), calls=%async_computation.3 | async-start | bytes 1310720 | tf_op jit(solution)/shard_map/all_gather | solution.py:156
  117.8 115.0 %all-gather.11.cloned.1.call-start = ((), (), s32[]{:S(2)}) async-start(), calls=%async_computation.4 | async-start | bytes 4718592 | tf_op jit(solution)/shard_map/all_gather | solution.py:162
  120.6 1.8 copy-start.5
  156.1 1.4 copy-start.1
  156.2 1.4 copy-start.3
  159.4 1.0 copy-start.2
  167.5 1.4 copy-start.1
  167.5 1.4 copy-start.3
  170.8 1.0 copy-start.2
  178.9 1.4 copy-start.1
  178.9 1.4 copy-start.3
  182.1 1.0 copy-start.2
  190.2 1.4 copy-start.1
  190.3 1.4 copy-start.3
  193.5 1.0 copy-start.2
  238.6 12.6 %copy-start.4 = (bf16[64,4096]{1,0:T(8,128)(2,1)S(1)}, bf16[64,4096]{1,0:T(8,128)(2,1)}, u32[]{:S(2)}) copy-start(bf16[64,4096]{1,0:T(8,128)(2,1)} %param.15) | copy-start | bytes 1572868
  238.6 12.6 %copy-start.6 = (f32[1,4096]{1,0:T(1,128)S(1)}, f32[1,4096]{1,0:T(1,128)}, u32[]{:S(2)}) copy-start(f32[1,4096]{1,0:T(1,128)} %get-tuple-element.90) | copy-start | bytes 49156
Sparse Core Ops, SparseCore 0:
  42.4 33.8 all-gather.4
  94.6 25.3 all-gather.6
  121.6 27.3 all-gather.8
  196.8 35.9 all-gather.10
where the time goes:
time: 260 us; the launch traced here: 259 us
  blocking collectives  71 us (27%)
  waiting for transfers between devices  57.7 us (22%)
  matrix products  51.5 us (20%)
  local copies, waits for them, and re-layouts  38.4 us (15%)
  other arithmetic  25.7 us (10%)
  between operations  13.4 us (5%)
    all_gather x1, waiting for transfers between devices, local(): lax.all_gather(attended, 'tp', axis=1, tiled=True)  36.1 us
    all_gather x1, waiting for transfers between devices, local(): lax.all_gather(values_here, 'sp', axis=0, tiled=True)  21.5 us
    psum x1, blocking collectives, local(): summed_mod = lax.psum(partial_mod, 'sp')  20.4 us
    dynamic_slice x12, local copies, waits for them, and re-layouts, sweep(): lax.scan(absorb_block, carry_state, (key_blocks, value_blocks))  18.9 us
    all_gather x1, blocking collectives, local(): lax.all_gather(own_keys, 'sp', axis=0, tiled=True)  14.6 us
    all_gather x1, blocking collectives, local(): lax.all_gather(own_values, 'sp', axis=0, tiled=True)  14.4 us
    all_to_all x1, blocking collectives, local(): lax.all_to_all(mixed_cols.astype(jnp.bfloat16), 'tp', split_axis=0, conca...  12.4 us
    dot_general x5, matrix products, absorb(): jnp.einsum('qhgd,khd->hgqk', grouped, key_heads, preferred_element_type=j...  11.9 us
  transfers between devices with their start and end apart: 4, of which 2 were waited for; matrix products, arithmetic and copies ran while one was open for 17% of the time, Pallas kernels for 0%

commit v1 on v0

--- a/solution.py
+++ b/solution.py
@@ -159,7 +159,7 @@
     attended = (numer / denom[..., None]).astype(jnp.bfloat16)
     attended = attended.transpose(2, 0, 1, 3).reshape(query_rows, query_cols)
     mixed_cols = jnp.dot(
-        lax.all_gather(attended, "tp", axis=1, tiled=True),
+        jnp.concatenate(lax.all_gather(attended, "tp"), axis=1),
         out_weight,
         preferred_element_type=jnp.float32,
     )

time: 260 us -> 234 us (0.900)
  local copies, waits for them, and re-layouts: 38.4 us -> 17.6 us
  waiting for transfers between devices: 57.7 us -> 69.4 us
  matrix products: 51.5 us -> 42.9 us
  other arithmetic: 25.7 us -> 18.8 us
    dynamic_slice x12, local copies, waits for them, and re-layouts: 18.9 us -> 5.08 us  [sweep(): lax.scan(absorb_block, carry_state, (key_blocks, value_blocks))]
    all_gather x0 -> x1, local copies, waits for them, and re-layouts: none -> 6.53 us  [local(): lax.all_gather(attended, 'tp')]
    all_gather x1, waiting for transfers between devices: 21.5 us -> 27.4 us  [local(): lax.all_gather(values_here, 'sp', axis=0, tiled=True)]
    all_gather x1, waiting for transfers between devices: 0.01 us -> 5.75 us  [local(): lax.all_gather(keys_here, 'sp', axis=0, tiled=True)]
    dot_general x5, matrix products: 11.9 us -> 6.72 us  [absorb(): jnp.einsum('qhgd,khd->hgqk', grouped, key_heads, preferred_element_type=j...]
    while x28 -> x4, local copies, waits for them, and re-layouts: 3.93 us -> 0.01 us
  transfers between devices with their start and end apart: 4 -> 4, of which waited for: 2 -> 3; matrix products, arithmetic and copies ran while one was open for 17% -> 12% of each run, Pallas kernels for 0% -> 0%
where the time goes in v1:
time: 234 us; the launch traced here: 233 us
  blocking collectives  70.3 us (30%)
  waiting for transfers between devices  69.4 us (30%)
  matrix products  42.9 us (18%)
  other arithmetic  18.8 us (8%)
  local copies, waits for them, and re-layouts  17.6 us (8%)
  between operations  13.5 us (6%)
    all_gather x1, waiting for transfers between devices, local(): lax.all_gather(attended, 'tp')  36.1 us
    all_gather x1, waiting for transfers between devices, local(): lax.all_gather(values_here, 'sp', axis=0, tiled=True)  27.4 us
    psum x1, blocking collectives, local(): summed_mod = lax.psum(partial_mod, 'sp')  20.4 us
    all_gather x1, blocking collectives, local(): lax.all_gather(own_values, 'sp', axis=0, tiled=True)  14.4 us
    all_gather x1, blocking collectives, local(): lax.all_gather(own_keys, 'sp', axis=0, tiled=True)  13.8 us
    all_to_all x1, blocking collectives, local(): lax.all_to_all(mixed_cols.astype(jnp.bfloat16), 'tp', split_axis=0, conca...  12.4 us
    dot_general x5, matrix products, absorb(): jnp.einsum('hgqk,khd->hgqd', expo.astype(jnp.bfloat16), value_heads, pref...  9.4 us
    all_gather x1, blocking collectives, local(): modulation = lax.all_gather(summed_mod, 'tp', axis=1, tiled=True)  9.23 us
  transfers between devices with their start and end apart: 4, of which 3 were waited for; matrix products, arithmetic and copies ran while one was open for 12% of the time, Pallas kernels for 0%

profile of v1, /device:TPU:0, one launch (start us, length us, event | category | flops | bytes accessed | tf_op | source)
XLA Modules:
  0.0 233.3 jit_solution(12828762995247617103)
XLA Ops:
  6.6 1.4 fusion.24
  8.0 0.6 copy-done
  8.6 1.2 fusion.36
  9.8 20.4 %psum.7 = f32[2,1536]{1,0:T(2,128)S(1)} all-reduce(f32[2,1536]{1,0:T(2,128)S(1)} %fusion.36), channel_id=1, replica_groups=mesh['sp'=4,'tp'=8] {'sp'}, use_global_device_ids=true, to_apply=%region_0.1 | all-reduce | flops 3072 | bytes 24576 | tf_op jit(solution)/shard_map/psum | solution.py:67
  30.3 9.2 %all_gather.21 = f32[2,12288]{1,0:T(2,128)S(1)} all-gather(f32[2,1536]{1,0:T(2,128)S(1)} %psum.7), channel_id=1, replica_groups=mesh['sp'=4,'tp'=8] {'tp'}, dimensions={1}, use_global_device_ids=true | all-gather | bytes 110592 | tf_op jit(solution)/shard_map/all_gather | solution.py:68
  39.6 2.2 fusion.28
  42.2 1.5 fusion.16
  43.8 2.5 %convolution_convert_fusion.2 = bf16[128,256]{1,0:T(8,128)(2,1)S(1)} fusion(bf16[4096,256]{1,0:T(8,128)(2,1)} %param.23, bf16[128,4096]{1,0:T(8,128)(2,1)} %param.16, f32[4096]{0:T(1024)S(1)} %bitcast.150, f32[4096]{0:T(1024)S(1)} %bitcast.152, f32[4096]{0:T(1024)S(1)} %copy-done.4, f32[128]{0:T(128)S(1)} %add_rsqrt_fusion.4), kind=kOutput, calls=%fused_computation.34 | convolution fusion | flops 271613952 | bytes 3260928 | tf_op jit(solution)/shard_map/dot_general | solution.py:102
  46.3 14.4 %all_gather.24 = bf16[512,256]{1,0:T(8,128)(2,1)S(1)} all-gather(bf16[128,256]{1,0:T(8,128)(2,1)S(1)} %convolution_convert_fusion.2), channel_id=1, replica_groups=mesh['sp'=4,'tp'=8] {'sp'}, dimensions={0}, use_global_device_ids=true | all-gather | bytes 327680 | tf_op jit(solution)/shard_map/all_gather | solution.py:107
  60.9 2.2 fusion.49
  63.4 13.8 %all_gather.22 = bf16[512,256]{1,0:T(8,128)(2,1)S(1)} all-gather(bf16[128,256]{1,0:T(8,128)(2,1)S(1)} %multiply_convert_fusion), channel_id=1, replica_groups=mesh['sp'=4,'tp'=8] {'sp'}, dimensions={0}, use_global_device_ids=true | all-gather | bytes 327680 | tf_op jit(solution)/shard_map/all_gather | solution.py:106
  77.4 0.2 fusion.31
  77.7 4.2 %bitcast_reduce_fusion.3 = (f32[512,4]{0,1:T(4,128)S(1)}, f32[512,256]{0,1:T(8,128)S(1)}) fusion(bf16[512,4096]{1,0:T(8,128)(2,1)} %all-gather.5.cloned.1.call-done, bf16[4096,256]{1,0:T(8,128)(2,1)} %param.22), kind=kOutput, calls=%fused_computation.46 | convolution fusion | flops 1074001920 | bytes 6823936 | tf_op jit(solution)/shard_map/dot_general | solution.py:74
  81.9 0.3 reshape.210
  82.2 0.3 multiply_multiply_fusion.1
  82.5 0.7 subtract_convert_fusion.1
  83.2 0.5 pad_maximum_fusion.1
  83.7 0.8 convert_element_type.83
  84.6 0.2 all-gather.9.cloned.1.call-start
  84.8 5.8 %bitcast_reduce_fusion.2 = (f32[512,8]{0,1:T(8,128)S(1)}, f32[512,512]{0,1:T(8,128)S(1)}) fusion(bf16[512,4096]{1,0:T(8,128)(2,1)} %all-gather.5.cloned.1.call-done, bf16[4096,512]{1,0:T(8,128)(2,1)} %param.21), kind=kOutput, calls=%fused_computation.41 | convolution fusion | flops 2148003840 | bytes 9453568 | tf_op jit(solution)/shard_map/dot_general | solution.py:73
  90.6 0.6 reshape.208
  91.3 0.5 multiply_multiply_fusion
  91.8 1.4 subtract_convert_fusion
  93.2 1.2 pad_maximum_fusion
  94.4 0.2 convert_element_type.80
  94.6 4.8 %convolution_convert_fusion.1 = bf16[512,256]{1,0:T(8,128)(2,1)} fusion(bf16[512,4096]{1,0:T(8,128)(2,1)} %all-gather.5.cloned.1.call-done, bf16[4096,256]{1,0:T(8,128)(2,1)} %param.23), kind=kOutput, calls=%fused_computation.33 | convolution fusion | flops 1073872896 | bytes 6553600 | tf_op jit(solution)/shard_map/dot_general | solution.py:75
  99.4 0.3 all-gather.11.cloned.1.call-start
  99.7 1.5 bitcast_reduce_fusion.1
  101.2 1.7 fusion.13
  102.9 2.1 fusion.21
  105.1 5.7 %all-gather.7.cloned.1.call-done = bf16[2048,256]{0,1:T(8,128)(2,1)} async-done(((bf16[512,256]{0,1:T(8,128)(2,1)}), bf16[2048,256]{0,1:T(8,128)(2,1)}) %all-gather.7.cloned.1.call-update) | async-done | bytes 1048592 | tf_op jit(solution)/shard_map/all_gather | solution.py:155
  110.8 1.5 copy.57
  112.3 27.4 %all-gather.9.cloned.1.call-done = bf16[2048,256]{1,0:T(8,128)(2,1)} async-done(((bf16[512,256]{1,0:T(8,128)(2,1)}), bf16[2048,256]{1,0:T(8,128)(2,1)}) %all-gather.9.cloned.1.call-update) | async-done | bytes 1048592 | tf_op jit(solution)/shard_map/all_gather | solution.py:156
  139.7 23.7 %while.14 = (s32[]{:T(128)}, f32[4,2,512]{2,1,0:T(2,128)S(1)}, f32[4,2,512]{2,1,0:T(2,128)S(1)}, f32[4,2,512,64]{2,3,1,0:T(8,128)S(1)}, bf16[4,512,256]{2,1,0:T(...) while((s32[]{:T(128)}, f32[4,2,512]{2,1,0:T(2,128)S(1)}, ...), condition=%wide.region_11.12_spmd, body=%wide.region_8.11_spmd.sunk | while | flops 554180608 | bytes 30670944 | solution.py:145
  139.7 1.0 constant_dynamic-slice_fusion.3
  140.7 0.1 copy.74
  140.9 0.1 copy.75
  141.0 1.3 bitcast_reduce_fusion.6
  142.4 1.4 fusion.77
  143.8 1.8 fusion.78
  145.7 1.0 constant_dynamic-slice_fusion.3
  146.6 0.1 copy.74
  146.8 0.1 copy.75
  146.9 1.3 bitcast_reduce_fusion.6
  148.3 1.4 fusion.77
  149.7 1.8 fusion.78
  151.6 1.0 constant_dynamic-slice_fusion.3
  152.6 0.1 copy.74
  152.7 0.1 copy.75
  152.9 1.3 bitcast_reduce_fusion.6
  154.2 1.4 fusion.77
  155.6 1.8 fusion.78
  157.5 1.0 constant_dynamic-slice_fusion.3
  158.5 0.1 copy.74
  158.6 0.1 copy.75
  158.8 1.3 bitcast_reduce_fusion.6
  160.1 1.4 fusion.77
  161.6 1.8 fusion.78
  163.5 1.0 copy.60
  164.6 36.1 %all-gather.11.cloned.1.call-done = bf16[8,512,512]{2,1,0:T(8,128)(2,1)} async-done(((bf16[1,512,512]{2,1,0:T(8,128)(2,1)}), bf16[8,512,512]{2,1,0:T(8,128)(2,1)}) %all-gather.11.cloned.1.call-update) | async-done | bytes 4194320 | tf_op jit(solution)/shard_map/all_gather | solution.py:162
  200.7 6.5 %copy.61 = bf16[8,512,512]{1,2,0:T(8,128)(2,1)} copy(bf16[8,512,512]{2,1,0:T(8,128)(2,1)} %all-gather.11.cloned.1.call-done) | data formatting | bytes 8388608 | tf_op jit(solution)/shard_map/all_gather | solution.py:162
  207.2 5.9 %convolution_convert_fusion = bf16[512,512]{1,0:T(8,128)(2,1)S(1)} fusion(bf16[512,4096]{0,1:T(8,128)(2,1)} %bitcast.134, bf16[4096,512]{1,0:T(8,128)(2,1)} %param.24), kind=kOutput, calls=%fused_computation.32 | convolution fusion | flops 2147745792 | bytes 8912896 | tf_op jit(solution)/shard_map/dot_general | solution.py:161
  213.2 12.4 %all_to_all.13 = bf16[8,64,512]{2,1,0:T(8,128)(2,1)S(1)} all-to-all(bf16[8,64,512]{2,1,0:T(8,128)(2,1)S(1)} %bitcast.144), channel_id=1, replica_groups=mesh['sp'=4,'tp'=8] {'tp'}, dimensions={0} | all-to-all | bytes 1048576 | tf_op jit(solution)/shard_map/all_to_all | solution.py:166
  225.8 0.9 fusion.29
  (59 shorter events, 1.7 us)
Async XLA Ops:
  6.5 2.1 copy-start
  6.5 37.2 %copy-start.4 = (f32[4096]{0:T(1024)S(1)}, f32[4096]{0:T(1024)}, u32[]{:S(2)}) copy-start(f32[4096]{0:T(1024)} %param.20) | copy-start | bytes 49156
  6.5 35.3 %copy-start.6 = (f32[8]{0:T(128)S(1)}, f32[8]{0:T(128)}, u32[]{:S(2)}) copy-start(f32[8]{0:T(128)} %param.27) | copy-start | bytes 100
  6.5 35.4 %copy-start.5 = (f32[64]{0:T(128)S(1)}, f32[64]{0:T(128)}, u32[]{:S(2)}) copy-start(f32[64]{0:T(128)} %param.26) | copy-start | bytes 772
  6.5 35.6 %copy-start.7 = (f32[64]{0:T(128)S(1)}, f32[64]{0:T(128)}, u32[]{:S(2)}) copy-start(f32[64]{0:T(128)} %param.25) | copy-start | bytes 772
  6.5 71.2 %all-gather.5.cloned.1.call-start = ((), (), s32[]{:S(2)}) async-start(), calls=%async_computation.1 | async-start | bytes 4718592 | tf_op jit(solution)/shard_map/all_gather | solution.py:71
  39.6 21.3 %copy-start.3 = (bf16[128,4096]{1,0:T(8,128)(2,1)S(1)}, bf16[128,4096]{1,0:T(8,128)(2,1)}, u32[]{:S(2)}) copy-start(bf16[128,4096]{1,0:T(8,128)(2,1)} %param.16) | copy-start | bytes 3145732
  41.8 69.0 %all-gather.7.cloned.1.call-start = ((), (), s32[]{:S(2)}) async-start(), calls=%async_computation.2 | async-start | bytes 1310720 | tf_op jit(solution)/shard_map/all_gather | solution.py:155
  84.6 55.2 %all-gather.9.cloned.1.call-start = ((), (), s32[]{:S(2)}) async-start(), calls=%async_computation.3 | async-start | bytes 1310720 | tf_op jit(solution)/shard_map/all_gather | solution.py:156
  99.4 101.3 %all-gather.11.cloned.1.call-start = ((), (), s32[]{:S(2)}) async-start(), calls=%async_computation.4 | async-start | bytes 4718592 | tf_op jit(solution)/shard_map/all_gather | solution.py:162
  207.2 19.5 %copy-start.1 = (bf16[1024,1536]{1,0:T(8,128)(2,1)S(1)}, bf16[1024,1536]{1,0:T(8,128)(2,1)}, u32[]{:S(2)}) copy-start(bf16[1024,1536]{1,0:T(8,128)(2,1)} %param.19) | copy-start | bytes 9437188
  213.2 12.6 %copy-start.2 = (bf16[64,4096]{1,0:T(8,128)(2,1)S(1)}, bf16[64,4096]{1,0:T(8,128)(2,1)}, u32[]{:S(2)}) copy-start(bf16[64,4096]{1,0:T(8,128)(2,1)} %param.15) | copy-start | bytes 1572868
Sparse Core Ops, SparseCore 0:
  41.9 33.8 all-gather.4
  84.7 26.1 all-gather.6
  112.4 27.2 all-gather.8
  164.7 35.9 all-gather.10
